TPU v7x, 32 devices: a whole 2x2x4 slice. The times are simulated.
32 devices in a mesh: grp: 2 (over y), sp: 4 (over z), dp: 4 (over x, core).
Axes of the slice: x: 2, y: 2, z: 4, core: 2. Of those that a mesh axis runs over, the one named last changes fastest.
Arguments:
- queries: bfloat16 [8, 512, 16, 192], P(('grp', 'dp'), 'sp'), parts along dimension 0, may hold values from -41 to 41
- kv_latent: bfloat16 [8, 512, 512], P(('grp', 'dp'), 'sp'), parts along dimension 0, may hold values from -6 to 6
- rope_key: bfloat16 [8, 512, 64], P(('grp', 'dp'), 'sp'), parts along dimension 0, may hold values from -5.1 to 5.1
- kv_gain: float32 [512], replicated, may hold values from 0.1 to 1.9
- kv_weight: bfloat16 [512, 4096], P('dp', 'sp'), may hold values from -0.25 to 0.25
- out_weight: bfloat16 [2048, 2048], P(None, 'dp'), may hold values from -1 to 1
Outputs:
- mixed: bfloat16 [8, 512, 2048], P(('grp', 'dp'), 'sp'), parts along dimension 0
There are 2 independent parts, one for each index of `grp`. A program takes and returns all parts, laid end to end along the dimension named above; an argument that names none is the same for every part. Nothing has to cross between parts.
All inputs are finite; a program needn't handle non-finite values.
Results may differ from a plain program's by a relative error of at most 0.0075.
Values may be sent and summed in bfloat16 or wider, within the bound.
A program may use at most 64 MiB of HBM per device.

v0:
```python
import jax
import jax.numpy as jnp
from jax import lax
from jax.sharding import PartitionSpec as P

NOPE = 128
VD = 128


def rotate(values, positions):
    half = values.shape[-1] // 2
    inverse = jnp.power(10000.0, -jnp.arange(half, dtype=jnp.float32) * 2.0 / values.shape[-1])
    angle = positions.astype(jnp.float32)[..., None] * inverse
    first = values[..., :half].astype(jnp.float32)
    second = values[..., half:].astype(jnp.float32)
    cosine = jnp.cos(angle)
    sine = jnp.sin(angle)
    return jnp.concatenate(
        [first * cosine - second * sine, first * sine + second * cosine], axis=-1
    )


def attend(query_rot, key_value, key_rot):
    length, heads = (query_rot.shape[0], query_rot.shape[1])
    nope = query_rot.shape[2] - key_rot.shape[1]
    scale = query_rot.shape[2] ** (-0.5)
    content = key_value[:, :, :nope]
    values = key_value[:, :, nope:]
    shared = jnp.broadcast_to(key_rot[:, None, :], (length, heads, key_rot.shape[1]))
    keys = jnp.concatenate([content, shared], axis=-1)
    block = min(512, length)
    blocks = query_rot.reshape(length // block, block, heads, query_rot.shape[2])
    key_pos = jnp.arange(length, dtype=jnp.int32)

    def one_block(item):
        query_block, index = item
        scores = (
            jnp.einsum("qhd,khd->hqk", query_block, keys, preferred_element_type=jnp.float32)
            * scale
        )
        query_pos = index * block + jnp.arange(block, dtype=jnp.int32)
        kept = query_pos[:, None] >= key_pos[None, :]
        scores = jnp.where(kept[None], scores, -jnp.inf)
        top = jnp.max(scores, axis=-1, keepdims=True)
        expo = jnp.exp(scores - top)
        probs = (expo / jnp.sum(expo, axis=-1, keepdims=True)).astype(jnp.bfloat16)
        return jnp.einsum("hqk,khd->qhd", probs, values, preferred_element_type=jnp.float32).astype(
            jnp.bfloat16
        )

    result = lax.map(one_block, (blocks, jnp.arange(length // block, dtype=jnp.int32)))
    return result.reshape(length, heads, values.shape[2])


def body(queries, kv_latent, rope_key, kv_gain, kv_weight, out_weight):
    tok_rows = queries.shape[1]
    positions = lax.axis_index("sp") * tok_rows + jnp.arange(tok_rows, dtype=jnp.int32)
    latent32 = kv_latent[0].astype(jnp.float32)
    latent_n = (
        latent32
        * lax.rsqrt(jnp.mean(latent32 * latent32, axis=-1, keepdims=True) + 1e-06)
        * kv_gain
    ).astype(jnp.bfloat16)
    key_rot = rotate(rope_key[0], positions).astype(jnp.bfloat16)
    turned = rotate(queries[0, :, :, NOPE:], positions[:, None])
    query_rot = jnp.concatenate(
        [queries[0, :, :, :NOPE].astype(jnp.float32), turned], axis=-1
    ).astype(jnp.bfloat16)
    query_heads = lax.all_to_all(query_rot[None], "sp", split_axis=2, concat_axis=1, tiled=True)
    every_latent, every_key = (
        lax.all_gather(latent_n[None], "sp", axis=1, tiled=True),
        lax.all_gather(key_rot[None], "sp", axis=1, tiled=True),
    )
    whole_latent = every_latent[0]
    kv_heads = jnp.dot(
        whole_latent,
        lax.all_gather(kv_weight, "dp", axis=0, tiled=True),
        preferred_element_type=jnp.float32,
    ).astype(jnp.bfloat16)
    kv_heads = kv_heads.reshape(whole_latent.shape[0], kv_weight.shape[1] // (NOPE + VD), NOPE + VD)
    attended = attend(query_heads[0], kv_heads, every_key[0])
    returned = lax.all_to_all(attended[None], "sp", split_axis=1, concat_axis=2, tiled=True)
    flat_rows = returned.reshape(tok_rows, returned.shape[2] * returned.shape[3])
    mixed = jnp.dot(
        flat_rows,
        lax.all_gather(out_weight, "dp", axis=1, tiled=True),
        preferred_element_type=jnp.float32,
    ).astype(jnp.bfloat16)
    return mixed[None]


def solution(mesh):
    return jax.shard_map(
        body,
        mesh=mesh,
        in_specs=(
            P(("grp", "dp"), "sp", None, None),
            P(("grp", "dp"), "sp", None),
            P(("grp", "dp"), "sp", None),
            P(),
            P("dp", "sp"),
            P(None, "dp"),
        ),
        out_specs=P(("grp", "dp"), "sp", None),
        check_vma=False,
    )
```

profile of v0, /device:TPU:0, one launch (start us, length us, event | category | flops | bytes accessed | tf_op | source)
XLA Modules:
  0.0 100.5 jit_solution(13270757476425511561)
XLA Ops:
  6.5 0.0 copy-start
  6.5 0.0 copy-start.2
  6.5 0.0 all-gather.3.cloned.1.call-start
  6.5 0.7 all-gather.3.cloned.1.call-update
  7.3 0.0 all-gather.5.cloned.1.call-start
  7.3 0.7 all-gather.5.cloned.1.call-update
  8.0 1.1 %slice.33 = bf16[1,128,16,128]{1,3,0,2:T(8,128)(2,1)S(1)} slice(bf16[1,128,16,192]{1,3,0,2:T(8,128)(2,1)} %bitcast.45), slice={[0:1], [0:128], [0:16], [0:128]} | slice | bytes 1048576 | tf_op jit(solution)/shard_map/slice | solution.py:67
  9.1 0.9 fusion.29
  10.0 1.0 slice_bitcast_fusion
  11.0 0.1 fusion.23
  11.1 0.9 pad_maximum_fusion
  12.0 6.3 %all-to-all-start = ((bf16[1,128,16,192]{1,3,0,2:T(8,128)(2,1)}), bf16[1,128,16,192]{1,3,0,2:T(8,128)(2,1)S(1)}, u32[]{:S(2)}, u32[]{:S(2)}) async-start(bf16[1,128,16,192]{1,3,0,2:T(8,128)(2,1)} %pad_maximum_fusion), calls=%async_computation | async-start | bytes 1572864 | tf_op jit(solution)/shard_map/all_to_all | solution.py:69
  18.4 25.7 %all_gather.14 = bf16[1,512,64]{1,2,0:T(8,128)(2,1)S(1)} all-gather(bf16[1,128,64]{1,2,0:T(8,128)(2,1)S(1)} %pad_maximum_fusion.1), channel_id=1, replica_groups=mesh['grp'=2,'sp'=4,'dp'=4] {'sp'}, dimensions={1}, use_global_device_ids=true | all-gather | bytes 81920 | tf_op jit(solution)/shard_map/all_gather | solution.py:72
  44.1 0.8 iota_compare_fusion
  44.9 0.0 copy-done
  44.9 0.1 fusion.15
  45.0 0.0 copy-done.2
  45.0 0.1 fusion.17
  45.1 14.7 %all_gather.12 = bf16[1,512,512]{2,1,0:T(8,128)(2,1)S(1)} all-gather(bf16[1,128,512]{2,1,0:T(8,128)(2,1)S(1)} %fusion.17), channel_id=1, replica_groups=mesh['grp'=2,'sp'=4,'dp'=4] {'sp'}, dimensions={1}, use_global_device_ids=true | all-gather | bytes 655360 | tf_op jit(solution)/shard_map/all_gather | solution.py:71
  59.8 0.0 all-to-all-done
  59.8 0.6 copy.35
  60.4 0.3 squeeze.21
  60.7 0.0 all-gather.3.cloned.1.call-done
  60.7 1.9 %convolution_convert_fusion.1 = bf16[512,1024]{1,0:T(8,128)(2,1)S(1)} fusion(bf16[512,1024]{1,0:T(8,128)(2,1)} %all-gather.3.cloned.1.call-done, bf16[1,512,512]{2,1,0:T(8,128)(2,1)S(1)} %all_gather.12), kind=kOutput, calls=%fused_computation.11 | convolution fusion | flops 537395200 | bytes 2621440 | tf_op jit(solution)/shard_map/dot_general | solution.py:75
  62.7 0.0 copy-start.1
  62.7 0.5 copy.33
  63.3 0.8 fusion.9
  64.1 0.0 copy-done.1
  64.2 2.1 %fusion.33 = (f32[4,512]{1,0:T(4,128)S(1)}, f32[4,512,512]{1,2,0:T(8,128)S(1)}) fusion(f32[4,512,512]{1,2,0:T(8,128)S(1)} %fusion.9, pred[512,512]{0,1:T(8,128)(4,1)S(1)} %copy-done.1), kind=kOutput, calls=%fused_computation.58 | output fusion | flops 6291967 | bytes 8658944 | tf_op jit(solution)/shard_map/while/body/eval_jaxpr/sub | solution.py:45
  66.3 0.5 fusion.8
  66.8 0.3 copy.29
  67.1 13.6 %all_to_all.30 = bf16[1,512,4,128]{3,2,0,1:T(4,128)(2,1)S(1)} all-to-all(bf16[1,512,4,128]{3,2,0,1:T(4,128)(2,1)S(1)} %copy.29), channel_id=1, replica_groups=mesh['grp'=2,'sp'=4,'dp'=4] {'sp'}, dimensions={1} | all-to-all | bytes 1048576 | tf_op jit(solution)/shard_map/all_to_all | solution.py:82
  80.8 0.1 copy.30
  80.8 0.3 copy.31
  81.1 7.1 %all-gather.5.cloned.1.call-done = bf16[2048,2048]{1,0:T(8,128)(2,1)} async-done(((bf16[2048,512]{1,0:T(8,128)(2,1)}), bf16[2048,2048]{1,0:T(8,128)(2,1)}) %all-gather.5.cloned.1.call-update) | async-done | bytes 8388624 | tf_op jit(solution)/shard_map/all_gather | solution.py:86
  88.2 5.5 %fusion.2 = bf16[1,128,2048]{2,1,0:T(8,128)(2,1)} fusion(bf16[128,2048]{0,1:T(8,128)(2,1)S(1)} %bitcast.39, bf16[2048,2048]{1,0:T(8,128)(2,1)} %all-gather.5.cloned.1.call-done), kind=kOutput, calls=%fused_computation.6 | convolution fusion | flops 1074003968 | bytes 9437184 | tf_op jit(solution)/shard_map/dot_general | solution.py:84
  (6 shorter events, 0.1 us)
Async XLA Ops:
  6.5 38.3 %copy-start = (bf16[1,128,512]{2,1,0:T(8,128)(2,1)S(1)}, bf16[1,128,512]{2,1,0:T(8,128)(2,1)}, u32[]{:S(2)}) copy-start(bf16[1,128,512]{2,1,0:T(8,128)(2,1)} %param.7) | copy-start | bytes 393220
  6.5 38.5 %copy-start.2 = (f32[512]{0:T(512)S(1)}, f32[512]{0:T(512)}, u32[]{:S(2)}) copy-start(f32[512]{0:T(512)} %param.9) | copy-start | bytes 6148
  6.5 54.2 %all-gather.3.cloned.1.call-start = ((), (), s32[]{:S(2)}) async-start(), calls=%async_computation.2 | async-start | bytes 1310720 | tf_op jit(solution)/shard_map/all_gather | solution.py:77
  7.3 80.9 %all-gather.5.cloned.1.call-start = ((), (), s32[]{:S(2)}) async-start(), calls=%async_computation.3 | async-start | bytes 10485760 | tf_op jit(solution)/shard_map/all_gather | solution.py:86
  12.0 47.8 %all-to-all-start = ((bf16[1,128,16,192]{1,3,0,2:T(8,128)(2,1)}), bf16[1,128,16,192]{1,3,0,2:T(8,128)(2,1)S(1)}, u32[]{:S(2)}, u32[]{:S(2)}) async-start(bf16[1,128,16,192]{1,3,0,2:T(8,128)(2,1)} %pad_maximum_fusion), calls=%async_computation | async-start | bytes 1572864 | tf_op jit(solution)/shard_map/all_to_all | solution.py:69
  62.7 1.5 %copy-start.1 = (pred[512,512]{0,1:T(8,128)(4,1)S(1)}, pred[512,512]{0,1:T(8,128)(4,1)}, u32[]{:S(2)}) copy-start(pred[512,512]{0,1:T(8,128)(4,1)} %iota_compare_fusion) | copy-start | bytes 786436
Sparse Core Ops, SparseCore 0:
  8.9 19.4 all-gather.2
  29.9 58.2 all-gather.4
where the time goes:
time: 101 us; the launch traced here: 100 us
  blocking collectives  54 us (53%)
  between operations  13.6 us (13%)
  matrix products  8.7 us (9%)
  waiting for transfers between devices  8.51 us (8%)
  starting transfers between devices  6.39 us (6%)
  other arithmetic  5.05 us (5%)
  local copies, waits for them, and re-layouts  4.24 us (4%)
    all_gather x1, blocking collectives, body(): lax.all_gather(key_rot[None], 'sp', axis=1, tiled=True)  25.7 us
    all_gather x1, blocking collectives, body(): lax.all_gather(latent_n[None], 'sp', axis=1, tiled=True)  14.7 us
    all_to_all x1, blocking collectives, body(): lax.all_to_all(attended[None], 'sp', split_axis=1, concat_axis=2, tiled=T...  13.6 us
    all_gather x1, waiting for transfers between devices, body(): lax.all_gather(out_weight, 'dp', axis=1, tiled=True)  7.08 us
    all_to_all x1, starting transfers between devices, body(): lax.all_to_all(query_rot[None], 'sp', split_axis=2, concat_axis=1, tiled=...  6.35 us
    dot_general x1, matrix products, body(): jnp.dot(flat_rows, lax.all_gather(out_weight, 'dp', axis=1, tiled=True),...  5.45 us
    sub x1, other arithmetic, one_block(): expo = jnp.exp(scores - top)  2.15 us
  transfers between devices with their start and end apart: 3, of which 1 were waited for; matrix products, arithmetic and copies ran while one was open for 12% of the time, Pallas kernels for 0%

commit v1 on v0

v1 whole, which is shorter than its diff:
```python
import functools

import jax
import jax.numpy as jnp
from jax import lax
from jax.experimental import pallas as pl
from jax.experimental.pallas import tpu as pltpu
from jax.sharding import PartitionSpec as P

NOPE = 128
VD = 128
LANES = 128
CORES = 2
CHUNKS = 8
MESH = pl.DeviceIdType.MESH


def rotate(values, positions):
    half = values.shape[-1] // 2
    inverse = jnp.power(10000.0, -jnp.arange(half, dtype=jnp.float32) * 2.0 / values.shape[-1])
    angle = positions.astype(jnp.float32)[..., None] * inverse
    first = values[..., :half].astype(jnp.float32)
    second = values[..., half:].astype(jnp.float32)
    cosine = jnp.cos(angle)
    sine = jnp.sin(angle)
    return jnp.concatenate(
        [first * cosine - second * sine, first * sine + second * cosine], axis=-1
    )


def kernel(
    n, g, nx, hn, rope, scale, chunks,
    q_ref, lat_ref, kvw_ref, w_ref, out_ref,
    qbuf, lat, kvw, wfull, kcat, vbuf, attsend, attrecv, acc,
    loc, q_s, q_r, a_s, a_r, lr_s, lr_r, rl_s, rl_r,
    kx_s, kx_r, kc_s, kc_r, wx_s, wx_r, wy_s, wy_r, wc_s, wc_r, wo_s, wo_r,
):
    me = lax.axis_index("sp")
    y = lax.axis_index("grp")
    dp = lax.axis_index("dp")
    x, c = dp // CORES, dp % CORES
    ndp = nx * CORES
    tok = lat_ref.shape[0]
    latw = kvw.shape[0]
    length = n * tok
    krows = kvw_ref.shape[0]
    part = w_ref.shape[0] // g
    crow = part // chunks
    cols = w_ref.shape[1]
    kd = hn * VD
    per_tile = LANES // rope

    def chip(xx, cc):
        return {"dp": xx * CORES + cc}

    partner = chip(x, 1 - c)

    def remote(src, dst, ss, rs, dev):
        return pltpu.make_async_remote_copy(
            src_ref=src, dst_ref=dst, send_sem=ss, recv_sem=rs, device_id=dev, device_id_type=MESH
        )

    own_w = pltpu.make_async_copy(w_ref, wfull.at[dp], loc.at[0])
    own_k = pltpu.make_async_copy(
        kvw_ref, kvw.at[pl.ds(pl.multiple_of(dp * krows, krows), krows)], loc.at[1]
    )
    own_q = pltpu.make_async_copy(q_ref.at[me], qbuf.at[me], loc.at[2])
    own_l = pltpu.make_async_copy(lat_ref, lat.at[me], loc.at[3])
    for copy in (own_k, own_q, own_l, own_w):
        copy.start()

    barrier = pltpu.get_barrier_semaphore()
    for o in range(1, n):
        pl.semaphore_signal(barrier, 1, device_id={"sp": lax.rem(me + o, n)}, device_id_type=MESH)
    for o in range(1, nx):
        pl.semaphore_signal(barrier, 1, device_id=chip(lax.rem(x + o, nx), c), device_id_type=MESH)
    for o in range(1, g):
        pl.semaphore_signal(barrier, 1, device_id={"grp": lax.rem(y + o, g)}, device_id_type=MESH)
    pl.semaphore_signal(barrier, 1, device_id=partner, device_id_type=MESH)
    pl.semaphore_wait(barrier, (n - 1) + (nx - 1) + (g - 1) + 1)

    def to_right(k, src):
        j = me - k
        return remote(src, lat.at[j], lr_s.at[k], lr_r.at[k], {"sp": me + 1})

    def to_left(k, src):
        j = me + k
        return remote(src, lat.at[j], rl_s.at[k], rl_r.at[k], {"sp": me - 1})

    @pl.when(me < n - 1)
    def _():
        to_right(0, lat_ref).start()

    @pl.when(me > 0)
    def _():
        to_left(0, lat_ref).start()

    def kv_rows(d):
        return kvw.at[pl.ds(pl.multiple_of(d * krows, krows), krows)]

    def kv_x(o):
        return remote(kvw_ref, kv_rows(dp), kx_s.at[o - 1], kx_r.at[o - 1], chip(lax.rem(x + o, nx), c))

    def kv_core(o):
        d = lax.rem(x + nx - o, nx) * CORES + c
        src = kvw_ref if o == 0 else kv_rows(d)
        return remote(src, kv_rows(d), kc_s.at[o], kc_r.at[o], partner)

    for o in range(1, nx):
        kv_x(o).start()
    kv_core(0).start()

    def q_copy(o):
        to = lax.rem(me + o, n)
        return remote(q_ref.at[to], qbuf.at[me], q_s.at[o], q_r.at[o], {"sp": to})

    for o in range(1, n):
        q_copy(o).start()

    def w_rows(yy, ch):
        return pl.ds(pl.multiple_of(yy * part + ch * crow, crow), crow)

    def w_x(o, ch):
        rows = w_rows(y, ch)
        return remote(
            w_ref.at[rows], wfull.at[dp, rows], wx_s.at[o - 1, ch], wx_r.at[o - 1, ch],
            chip(lax.rem(x + o, nx), c),
        )

    def w_y(o, p, ch):
        ref = wfull.at[lax.rem(x + nx - o, nx) * CORES + c, w_rows(y, ch)]
        return remote(
            ref, ref, wy_s.at[o - 1, p - 1, ch], wy_r.at[o - 1, p - 1, ch],
            {"grp": lax.rem(y + p, g)},
        )

    def w_c(o, p, ch):
        ref = wfull.at[lax.rem(x + nx - o, nx) * CORES + c, w_rows(lax.rem(y + g - p, g), ch)]
        return remote(ref, ref, wc_s.at[o - 1, p, ch], wc_r.at[o - 1, p, ch], partner)

    for ch in range(chunks):
        for o in range(1, nx):
            w_x(o, ch).start()
    w_own = remote(w_ref, wfull.at[dp], wo_s, wo_r, partner)
    w_own.start()

    own_l.wait()
    for k in range(1, n):
        @pl.when(me - k >= 0)
        def _():
            to_right(k - 1, lat_ref).wait_recv()

            @pl.when(me < n - 1)
            def _():
                to_right(k, lat.at[me - k]).start()

        @pl.when(me + k < n)
        def _():
            to_left(k - 1, lat_ref).wait_recv()

            @pl.when(me > 0)
            def _():
                to_left(k, lat.at[me + k]).start()

    for o in range(1, nx):
        kv_x(o).wait_recv()
        kv_core(o).start()
    own_k.wait()
    for o in range(nx):
        kv_core(o).wait_recv()

    lane = lax.broadcasted_iota(jnp.int32, (tok, LANES), 1)

    @pl.loop(0, n)
    def _(j):
        rows = pl.ds(pl.multiple_of(j * tok, tok), tok)
        shared = lat[j, :, latw:].astype(jnp.float32)
        spread = [
            jnp.where(lane // rope == i, shared, 0.0).astype(jnp.bfloat16) for i in range(per_tile)
        ]
        block = lat[j, :, :latw]
        for h in range(hn):
            wide = NOPE + VD
            both = jnp.dot(
                block, kvw[:, h * wide : (h + 1) * wide], preferred_element_type=jnp.float32
            ).astype(jnp.bfloat16)
            kcat[h, rows, :NOPE] = both[:, :NOPE]
            kcat[h, rows, NOPE:] = spread[h % per_tile]
            vbuf[h, rows, :] = both[:, NOPE:]

    def pass_x(ch):
        for o in range(1, nx):
            w_x(o, ch).wait_recv()
            for p in range(1, g):
                w_y(o, p, ch).start()
            w_c(o, 0, ch).start()

    def pass_y(ch):
        for o in range(1, nx):
            for p in range(1, g):
                w_y(o, p, ch).wait_recv()
                w_c(o, p, ch).start()

    def attention(j):
        col = lax.broadcasted_iota(jnp.int32, (tok, length), 1)
        row = lax.broadcasted_iota(jnp.int32, (tok, length), 0)
        kept = col - row <= j * tok
        for h in range(hn):
            query = jnp.concatenate([qbuf[j, h], qbuf[j, hn + h // per_tile]], axis=-1)
            s = lax.dot_general(
                query, kcat[h], (((1,), (1,)), ((), ())), preferred_element_type=jnp.float32
            ) * scale
            s = jnp.where(kept, s, -jnp.inf)
            top = jnp.max(s, axis=-1, keepdims=True)
            e = jnp.exp(s - top)
            p = (e * (1.0 / jnp.sum(e, axis=-1, keepdims=True))).astype(jnp.bfloat16)
            o = jnp.dot(p, vbuf[h], preferred_element_type=jnp.float32).astype(jnp.bfloat16)
            attsend[j, :, h * VD : (h + 1) * VD] = o

    def a_copy(o):
        to = lax.rem(me + n - o, n)
        return remote(attsend.at[to], attrecv.at[me], a_s.at[o], a_r.at[o], {"sp": to})

    own_q.wait()
    attention(me)
    own_a = pltpu.make_async_copy(attsend.at[me], attrecv.at[me], loc.at[4])
    own_a.start()

    per = -(-chunks // n)
    for b in range(min(per, chunks)):
        pass_x(b)

    @pl.loop(1, n)
    def _(o):
        q_copy(o).wait_recv()
        attention(lax.rem(me + n - o, n))
        a_copy(o).start()
        for b in range(per):
            ch = o * per + b

            @pl.when(ch < chunks)
            def _():
                pass_x(ch)

            @pl.when(ch - per < chunks)
            def _():
                pass_y(ch - per)

    for ch in range(chunks):
        if ch >= (n - 1) * per:
            pass_y(ch)

    own_w.wait()
    w_own.wait_recv()
    for o in range(1, nx):
        for p in range(g):
            for ch in range(chunks):
                w_c(o, p, ch).wait_recv()
    own_a.wait()

    def project(j, first):
        rows = pl.ds(pl.multiple_of(j * kd, kd), kd)
        block = attrecv[j]
        for d in range(ndp):
            part_sum = jnp.dot(block, wfull[d, rows, :], preferred_element_type=jnp.float32)
            if first:
                acc[:, d * cols : (d + 1) * cols] = part_sum
            else:
                acc[:, d * cols : (d + 1) * cols] += part_sum

    project(me, True)

    @pl.loop(1, n)
    def _(o):
        a_copy(o).wait_recv()
        project(lax.rem(me + o, n), False)

    out_ref[...] = acc[...].astype(out_ref.dtype)

    for k in range(n - 1):
        @pl.when((me - k >= 0) & (me < n - 1))
        def _():
            to_right(k, lat_ref).wait_send()

        @pl.when((me + k < n) & (me > 0))
        def _():
            to_left(k, lat_ref).wait_send()
    for o in range(1, n):
        q_copy(o).wait_send()
        a_copy(o).wait_send()
    w_own.wait_send()
    for o in range(nx):
        kv_core(o).wait_send()
    for o in range(1, nx):
        kv_x(o).wait_send()
        for ch in range(chunks):
            w_x(o, ch).wait_send()
            for p in range(1, g):
                w_y(o, p, ch).wait_send()
            for p in range(g):
                w_c(o, p, ch).wait_send()


def body(sizes, queries, kv_latent, rope_key, kv_gain, kv_weight, out_weight):
    g, n, dp = sizes
    nx = dp // CORES
    tok, heads, width = queries.shape[1:]
    rope = width - NOPE
    hn = heads // n
    latw = kv_latent.shape[2]
    positions = lax.axis_index("sp") * tok + jnp.arange(tok, dtype=jnp.int32)
    latent32 = kv_latent[0].astype(jnp.float32)
    latent_n = (
        latent32
        * lax.rsqrt(jnp.mean(latent32 * latent32, axis=-1, keepdims=True) + 1e-06)
        * kv_gain
    ).astype(jnp.bfloat16)
    key_rot = rotate(rope_key[0], positions).astype(jnp.bfloat16)
    packed = jnp.concatenate([latent_n] + [key_rot] * (LANES // rope), axis=1)
    turned = rotate(queries[0, :, :, NOPE:], positions[:, None]).astype(jnp.bfloat16)
    content = queries[0, :, :, :NOPE].reshape(tok, n, hn, NOPE).transpose(1, 2, 0, 3)
    tiles = -(-hn * rope // LANES)
    turned = turned.reshape(tok, n, hn * rope)
    turned = jnp.pad(turned, ((0, 0), (0, 0), (0, tiles * LANES - hn * rope)))
    turned = turned.reshape(tok, n, tiles, LANES).transpose(1, 2, 0, 3)
    q = jnp.concatenate([content, turned], axis=1)

    d_in, cols = out_weight.shape
    part = d_in // g
    chunks = CHUNKS
    kcols = kv_weight.shape[1]
    dma = pltpu.SemaphoreType.DMA
    bf = jnp.bfloat16
    xn = max(nx - 1, 1)
    gn = max(g - 1, 1)
    vmem = pl.BlockSpec(memory_space=pltpu.VMEM)
    out = pl.pallas_call(
        functools.partial(kernel, n, g, nx, hn, rope, width**-0.5, chunks),
        out_shape=jax.ShapeDtypeStruct((tok, cols * dp), bf),
        in_specs=[vmem, vmem, vmem, pl.BlockSpec(memory_space=pltpu.HBM)],
        out_specs=vmem,
        scratch_shapes=[
            pltpu.VMEM((n, hn + tiles, tok, LANES), bf),
            pltpu.VMEM((n, tok, latw + LANES), bf),
            pltpu.VMEM((kv_weight.shape[0] * dp, kcols), bf),
            pltpu.VMEM((dp, d_in, cols), bf),
            pltpu.VMEM((hn, n * tok, NOPE + LANES), bf),
            pltpu.VMEM((hn, n * tok, VD), bf),
            pltpu.VMEM((n, tok, hn * VD), bf),
            pltpu.VMEM((n, tok, hn * VD), bf),
            pltpu.VMEM((tok, cols * dp), jnp.float32),
            dma((5,)),
            dma((n,)), dma((n,)), dma((n,)), dma((n,)),
            dma((n,)), dma((n,)), dma((n,)), dma((n,)),
            dma((xn,)), dma((xn,)), dma((nx,)), dma((nx,)),
            dma((xn, chunks)), dma((xn, chunks)),
            dma((xn, gn, chunks)), dma((xn, gn, chunks)),
            dma((xn, g, chunks)), dma((xn, g, chunks)),
            dma(()), dma(()),
        ],
        compiler_params=pltpu.CompilerParams(
            collective_id=0, has_side_effects=True, vmem_limit_bytes=56 * 1024 * 1024
        ),
    )(q, packed, kv_weight, out_weight)
    return out[None]


def solution(mesh):
    sizes = (mesh.shape["grp"], mesh.shape["sp"], mesh.shape["dp"])
    return jax.shard_map(
        functools.partial(body, sizes),
        mesh=mesh,
        in_specs=(
            P(("grp", "dp"), "sp", None, None),
            P(("grp", "dp"), "sp", None),
            P(("grp", "dp"), "sp", None),
            P(),
            P("dp", "sp"),
            P(None, "dp"),
        ),
        out_specs=P(("grp", "dp"), "sp", None),
        check_vma=False,
    )
```

time: 101 us -> 75.9 us (0.75)
  Pallas kernels: 0 us -> 68.7 us
  blocking collectives: 54 us -> 0 us
  between operations: 13.6 us -> 0.11 us
  matrix products: 8.7 us -> 0 us
  waiting for transfers between devices: 8.51 us -> 0 us
  starting transfers between devices: 6.39 us -> 0 us
  other arithmetic: 5.05 us -> 1.62 us
    pallas_call x0 -> x1, Pallas kernels: none -> 68.7 us  [body(): pl.pallas_call(functools.partial(kernel, n, g, nx, hn, rope, width ** (-0...]
    all_gather x2 -> x0, blocking collectives: 40.4 us -> none  [the longest x1 25.7 us: body(): lax.all_gather(key_rot[None], 'sp', axis=1, tiled=True)]
    all_to_all x1 -> x0, blocking collectives: 13.6 us -> none  [body(): lax.all_to_all(attended[None], 'sp', split_axis=1, concat_axis=2, tiled=T...]
    dot_general x4 -> x0, matrix products: 8.7 us -> none  [the longest x1 5.45 us: body(): jnp.dot(flat_rows, lax.all_gather(out_weight, 'dp', axis=1, tiled=True),...]
    all_gather x2 -> x0, waiting for transfers between devices: 7.1 us -> none  [the longest x1 7.08 us: body(): lax.all_gather(out_weight, 'dp', axis=1, tiled=True)]
    all_to_all x1 -> x0, starting transfers between devices: 6.35 us -> none  [body(): lax.all_to_all(query_rot[None], 'sp', split_axis=2, concat_axis=1, tiled=...]
    unnamed x6, local copies, waits for them, and re-layouts: 0.01 us -> 2.78 us
    sub x1 -> x0, other arithmetic: 2.15 us -> none  [one_block(): expo = jnp.exp(scores - top)]
  transfers between devices with their start and end apart: 3 -> 0, of which waited for: 1 -> 0; matrix products, arithmetic and copies ran while one was open for 12% -> 0% of each run, Pallas kernels for 0% -> 0%
where the time goes in v1:
time: 75.9 us; the launch traced here: 75.6 us
  Pallas kernels  68.7 us (91%)
  local copies, waits for them, and re-layouts  5.14 us (7%)
  other arithmetic  1.62 us (2%)
    pallas_call x1, Pallas kernels, body(): pl.pallas_call(functools.partial(kernel, n, g, nx, hn, rope, width ** (-0...  68.7 us
    unnamed x6, local copies, waits for them, and re-layouts  2.78 us

profile of v1, /device:TPU:0, one launch (start us, length us, event | category | flops | bytes accessed | tf_op | source)
XLA Modules:
  0.0 75.6 jit_solution(9956832551271919494)
XLA Ops:
  0.0 0.0 slice-start
  0.0 0.9 %copy.21 = bf16[1,128,64]{2,1,0:T(8,128)(2,1)S(1)} copy(bf16[1,128,64]{1,2,0:T(8,128)(2,1)} %param.8) | data formatting | bytes 32768 | tf_op args[2]
  0.9 0.3 fusion.10
  1.2 0.1 copy.18
  1.3 0.1 copy.19
  1.4 1.0 %slice_bitcast_fusion = bf16[128,16,64]{0,2,1:T(8,128)(2,1)S(1)} fusion(bf16[1,128,16,192]{1,3,2,0:T(8,128)(2,1)} %param.6), kind=kLoop, calls=%fused_computation.15 | loop fusion | bytes 524288 | tf_op jit(solution)/shard_map/squeeze | solution.py:320
  2.4 0.1 fusion.1
  2.5 0.0 copy-start
  2.5 0.0 copy-start.1
  2.5 0.2 copy.20
  2.7 0.0 slice-done
  2.7 0.3 copy.16
  3.0 1.0 %pad_maximum_fusion.q_ref = bf16[4,6,128,128]{3,2,1,0:T(8,128)(2,1)} fusion(bf16[4,2,128,128]{3,2,1,0:T(8,128)(2,1)S(1)} %bitcast.16, bf16[4,4,128,128]{3,2,1,0:T(8,128)(2,1)S(1)} %bitcast.13), kind=kLoop, calls=%fused_computation | loop fusion | flops 393216 | bytes 1572864 | tf_op jit(solution)/shard_map/concatenate | solution.py:326
  4.0 0.0 copy-done
  4.0 0.1 fusion.4
  4.1 0.0 copy-done.1
  4.1 0.1 fusion.6
  4.2 0.8 %concatenate.15.lat_ref = bf16[128,640]{1,0:T(8,128)(2,1)} concatenate(bf16[128,512]{1,0:T(8,128)(2,1)S(1)} %fusion.6, bf16[128,32]{1,0:T(8,128)(2,1)S(1)} %get-tuple-element.8, bf16[128,32]{1,0:T(8,128)(2,1)S(1)} %get-tuple-element.7, bf16[128,32]{1,0:T(8,128)(2,1)S(1)} %get-tuple-element.8, bf16[128,32]{1,0:T(8,128)(2,1)S(1)} %get-tuple-element.7), dimensions={1} | concatenate | bytes 327680 | tf_op jit(solution)/shard_map/concatenate | solution.py:319
  5.0 68.7 %shard_map.64 = bf16[128,2048]{1,0:T(8,128)(2,1)} custom-call(bf16[4,6,128,128]{3,2,1,0:T(8,128)(2,1)} %pad_maximum_fusion.q_ref, bf16[128,640]{1,0:T(8,128)(2,1)} %concatenate.15.lat_ref, bf16[128,1024]{1,0:T(8,128)(2,1)} %kvw_ref.1, bf16[2048,512]{1,0:T(8,128)(2,1)} %w_ref.1), custom_call_target="tpu_custom_call" | custom-call | tf_op jit(solution)/shard_map/pallas_call | solution.py:337
  73.7 1.9 %copy.23 = bf16[1,128,2048]{2,1,0:T(8,128)(2,1)} copy(bf16[1,128,2048]{2,1,0:T(8,128)(2,1)} %bitcast.14) | data formatting | bytes 1048576
  (4 shorter events, 0.0 us)
Async XLA Ops:
  0.0 2.7 %slice-start = ((bf16[1,128,16,192]{1,3,2,0:T(8,128)(2,1)}), bf16[1,128,16,128]{1,3,2,0:T(8,128)(2,1)S(1)}, s32[]{:S(2)}) async-start(bf16[1,128,16,192]{1,3,2,0:T(8,128)(2,1)} %param.6), calls=%async_computation | async-start | bytes 1048576 | tf_op jit(solution)/shard_map/slice | solution.py:321
  2.5 1.5 %copy-start = (bf16[1,128,512]{2,1,0:T(8,128)(2,1)S(1)}, bf16[1,128,512]{2,1,0:T(8,128)(2,1)}, u32[]{:S(2)}) copy-start(bf16[1,128,512]{2,1,0:T(8,128)(2,1)} %param.7) | copy-start | bytes 393220
  2.5 1.6 %copy-start.1 = (f32[512]{0:T(512)S(1)}, f32[512]{0:T(512)}, u32[]{:S(2)}) copy-start(f32[512]{0:T(512)} %param.9) | copy-start | bytes 6148

commit v2 on v1

--- a/solution.py
+++ b/solution.py
@@ -1,7 +1,9 @@
 import functools
+import math
 
 import jax
 import jax.numpy as jnp
+import numpy as np
 from jax import lax
 from jax.experimental import pallas as pl
 from jax.experimental.pallas import tpu as pltpu
@@ -15,22 +17,19 @@
 MESH = pl.DeviceIdType.MESH
 
 
-def rotate(values, positions):
-    half = values.shape[-1] // 2
-    inverse = jnp.power(10000.0, -jnp.arange(half, dtype=jnp.float32) * 2.0 / values.shape[-1])
-    angle = positions.astype(jnp.float32)[..., None] * inverse
-    first = values[..., :half].astype(jnp.float32)
-    second = values[..., half:].astype(jnp.float32)
-    cosine = jnp.cos(angle)
-    sine = jnp.sin(angle)
-    return jnp.concatenate(
-        [first * cosine - second * sine, first * sine + second * cosine], axis=-1
-    )
+VARIANTS = 4
+
+
+def rotation_table(length, rope):
+    half = rope // 2
+    inverse = np.power(10000.0, -np.arange(half) * 2.0 / rope).astype(np.float32)
+    angle = inverse[:, None] * np.arange(length, dtype=np.float32)[None, :]
+    return np.stack([np.cos(angle), np.sin(angle)]).astype(np.float32)
 
 
 def kernel(
     n, g, nx, hn, rope, scale, chunks,
-    q_ref, lat_ref, kvw_ref, w_ref, out_ref,
+    q_ref, latent_ref, key_ref, gain_ref, table_ref, kvw_ref, w_ref, out_ref,
     qbuf, lat, kvw, wfull, kcat, vbuf, attsend, attrecv, acc,
     loc, q_s, q_r, a_s, a_r, lr_s, lr_r, rl_s, rl_r,
     kx_s, kx_r, kc_s, kc_r, wx_s, wx_r, wy_s, wy_r, wc_s, wc_r, wo_s, wo_r,
@@ -40,7 +39,9 @@
     dp = lax.axis_index("dp")
     x, c = dp // CORES, dp % CORES
     ndp = nx * CORES
-    tok = lat_ref.shape[0]
+    tok = latent_ref.shape[0]
+    half = rope // 2
+    lat_ref = lat.at[me]
     latw = kvw.shape[0]
     length = n * tok
     krows = kvw_ref.shape[0]
@@ -48,7 +49,27 @@
     crow = part // chunks
     cols = w_ref.shape[1]
     kd = hn * VD
-    per_tile = LANES // rope
+
+    def xor(a, b):
+        total, bit = 0, 1
+        while bit < n:
+            total = total + bit * lax.rem(lax.div(a, bit) + lax.div(jnp.int32(b), bit), 2)
+            bit *= 2
+        return total
+
+    paired = n & (n - 1) == 0
+
+    def target(o):
+        return xor(me, o) if paired else lax.rem(me + o, n)
+
+    def source(o):
+        return xor(me, o) if paired else lax.rem(me + n - o, n)
+
+    def turned(values, j):
+        span = pl.ds(pl.multiple_of(j * tok, tok), tok)
+        cosine, sine = table_ref[0, :, span], table_ref[1, :, span]
+        first, second = values[:half].astype(jnp.float32), values[half:].astype(jnp.float32)
+        return first * cosine - second * sine, first * sine + second * cosine
 
     def chip(xx, cc):
         return {"dp": xx * CORES + cc}
@@ -64,9 +85,8 @@
     own_k = pltpu.make_async_copy(
         kvw_ref, kvw.at[pl.ds(pl.multiple_of(dp * krows, krows), krows)], loc.at[1]
     )
-    own_q = pltpu.make_async_copy(q_ref.at[me], qbuf.at[me], loc.at[2])
-    own_l = pltpu.make_async_copy(lat_ref, lat.at[me], loc.at[3])
-    for copy in (own_k, own_q, own_l, own_w):
+    own_q = pltpu.make_async_copy(q_ref.at[pl.ds(me * hn, hn)], qbuf.at[me], loc.at[2])
+    for copy in (own_k, own_q, own_w):
         copy.start()
 
     barrier = pltpu.get_barrier_semaphore()
@@ -77,6 +97,14 @@
     for o in range(1, g):
         pl.semaphore_signal(barrier, 1, device_id={"grp": lax.rem(y + o, g)}, device_id_type=MESH)
     pl.semaphore_signal(barrier, 1, device_id=partner, device_id_type=MESH)
+
+    latent = latent_ref[...].astype(jnp.float32)
+    square = jnp.mean(latent * latent, axis=-1, keepdims=True)
+    lat[me, :, :latw] = (latent * lax.rsqrt(square + 1e-06) * gain_ref[...]).astype(jnp.bfloat16)
+    first, second = turned(key_ref[...], me)
+    rest = jnp.zeros((LANES - rope, tok), jnp.float32)
+    lat[me, :, latw:] = jnp.concatenate([first, second, rest], axis=0).T.astype(jnp.bfloat16)
+
     pl.semaphore_wait(barrier, (n - 1) + (nx - 1) + (g - 1) + 1)
 
     def to_right(k, src):
@@ -111,8 +139,8 @@
     kv_core(0).start()
 
     def q_copy(o):
-        to = lax.rem(me + o, n)
-        return remote(q_ref.at[to], qbuf.at[me], q_s.at[o], q_r.at[o], {"sp": to})
+        to = target(o)
+        return remote(q_ref.at[pl.ds(to * hn, hn)], qbuf.at[me], q_s.at[o], q_r.at[o], {"sp": to})
 
     for o in range(1, n):
         q_copy(o).start()
@@ -144,7 +172,6 @@
     w_own = remote(w_ref, wfull.at[dp], wo_s, wo_r, partner)
     w_own.start()
 
-    own_l.wait()
     for k in range(1, n):
         @pl.when(me - k >= 0)
         def _():
@@ -169,24 +196,19 @@
     for o in range(nx):
         kv_core(o).wait_recv()
 
-    lane = lax.broadcasted_iota(jnp.int32, (tok, LANES), 1)
-
     @pl.loop(0, n)
     def _(j):
         rows = pl.ds(pl.multiple_of(j * tok, tok), tok)
-        shared = lat[j, :, latw:].astype(jnp.float32)
-        spread = [
-            jnp.where(lane // rope == i, shared, 0.0).astype(jnp.bfloat16) for i in range(per_tile)
-        ]
         block = lat[j, :, :latw]
+        shared = lat[j, :, latw:]
         for h in range(hn):
             wide = NOPE + VD
             both = jnp.dot(
                 block, kvw[:, h * wide : (h + 1) * wide], preferred_element_type=jnp.float32
-            ).astype(jnp.bfloat16)
-            kcat[h, rows, :NOPE] = both[:, :NOPE]
-            kcat[h, rows, NOPE:] = spread[h % per_tile]
-            vbuf[h, rows, :] = both[:, NOPE:]
+            )
+            kcat[h, rows, :NOPE] = both[:, :NOPE].astype(jnp.bfloat16)
+            kcat[h, rows, NOPE:] = shared
+            vbuf[h, :, rows] = both[:, NOPE:].T.astype(jnp.bfloat16)
 
     def pass_x(ch):
         for o in range(1, nx):
@@ -201,54 +223,64 @@
                 w_y(o, p, ch).wait_recv()
                 w_c(o, p, ch).start()
 
+    variants = math.gcd(VARIANTS, n)
+    step = length // variants
+
+    def attention_over(j, extent):
+        row = lax.broadcasted_iota(jnp.int32, (step, tok), 0)
+        col = lax.broadcasted_iota(jnp.int32, (step, tok), 1)
+        kept = row - col <= j * tok - (extent - step)
+        pad = jnp.zeros((LANES - rope, tok), jnp.bfloat16)
+        for h in range(hn):
+            first, second = turned(qbuf[j, h, NOPE:, :], j)
+            query = jnp.concatenate(
+                [qbuf[j, h, :NOPE, :], first.astype(jnp.bfloat16), second.astype(jnp.bfloat16), pad],
+                axis=0,
+            )
+            s = jnp.dot(kcat[h, :extent, :], query, preferred_element_type=jnp.float32)
+            last = jnp.where(kept, s[extent - step :], -jnp.inf)
+            s = last if extent == step else jnp.concatenate([s[: extent - step], last], axis=0)
+            top = jnp.max(s, axis=0, keepdims=True)
+            e = jnp.exp2((s - top) * (scale * math.log2(math.e)))
+            total = jnp.sum(e, axis=0, keepdims=True)
+            o = jnp.dot(vbuf[h, :, :extent], e.astype(jnp.bfloat16), preferred_element_type=jnp.float32)
+            attsend[j, :, h * VD : (h + 1) * VD] = (o / total).T.astype(jnp.bfloat16)
+
     def attention(j):
-        col = lax.broadcasted_iota(jnp.int32, (tok, length), 1)
-        row = lax.broadcasted_iota(jnp.int32, (tok, length), 0)
-        kept = col - row <= j * tok
-        for h in range(hn):
-            query = jnp.concatenate([qbuf[j, h], qbuf[j, hn + h // per_tile]], axis=-1)
-            s = lax.dot_general(
-                query, kcat[h], (((1,), (1,)), ((), ())), preferred_element_type=jnp.float32
-            ) * scale
-            s = jnp.where(kept, s, -jnp.inf)
-            top = jnp.max(s, axis=-1, keepdims=True)
-            e = jnp.exp(s - top)
-            p = (e * (1.0 / jnp.sum(e, axis=-1, keepdims=True))).astype(jnp.bfloat16)
-            o = jnp.dot(p, vbuf[h], preferred_element_type=jnp.float32).astype(jnp.bfloat16)
-            attsend[j, :, h * VD : (h + 1) * VD] = o
+        for v in range(variants):
+            @pl.when(j // (n // variants) == v)
+            def _():
+                attention_over(j, (v + 1) * step)
 
     def a_copy(o):
-        to = lax.rem(me + n - o, n)
+        to = source(o)
         return remote(attsend.at[to], attrecv.at[me], a_s.at[o], a_r.at[o], {"sp": to})
 
     own_q.wait()
-    attention(me)
-    own_a = pltpu.make_async_copy(attsend.at[me], attrecv.at[me], loc.at[4])
-    own_a.start()
-
     per = -(-chunks // n)
     for b in range(min(per, chunks)):
         pass_x(b)
 
-    @pl.loop(1, n)
+    @pl.loop(0, n)
     def _(o):
-        q_copy(o).wait_recv()
-        attention(lax.rem(me + n - o, n))
-        a_copy(o).start()
+        @pl.when(o > 0)
+        def _():
+            q_copy(o).wait_recv()
+
+        attention(source(o))
+
+        @pl.when(o > 0)
+        def _():
+            a_copy(o).start()
+
         for b in range(per):
-            ch = o * per + b
-
-            @pl.when(ch < chunks)
+            @pl.when((o + 1) * per + b < chunks)
             def _():
-                pass_x(ch)
-
-            @pl.when(ch - per < chunks)
+                pass_x((o + 1) * per + b)
+
+            @pl.when(o * per + b < chunks)
             def _():
-                pass_y(ch - per)
-
-    for ch in range(chunks):
-        if ch >= (n - 1) * per:
-            pass_y(ch)
+                pass_y(o * per + b)
 
     own_w.wait()
     w_own.wait_recv()
@@ -256,11 +288,10 @@
         for p in range(g):
             for ch in range(chunks):
                 w_c(o, p, ch).wait_recv()
-    own_a.wait()
 
     def project(j, first):
         rows = pl.ds(pl.multiple_of(j * kd, kd), kd)
-        block = attrecv[j]
+        block = attsend[me] if first else attrecv[j]
         for d in range(ndp):
             part_sum = jnp.dot(block, wfull[d, rows, :], preferred_element_type=jnp.float32)
             if first:
@@ -273,7 +304,7 @@
     @pl.loop(1, n)
     def _(o):
         a_copy(o).wait_recv()
-        project(lax.rem(me + o, n), False)
+        project(target(o), False)
 
     out_ref[...] = acc[...].astype(out_ref.dtype)
 
@@ -308,22 +339,9 @@
     rope = width - NOPE
     hn = heads // n
     latw = kv_latent.shape[2]
-    positions = lax.axis_index("sp") * tok + jnp.arange(tok, dtype=jnp.int32)
-    latent32 = kv_latent[0].astype(jnp.float32)
-    latent_n = (
-        latent32
-        * lax.rsqrt(jnp.mean(latent32 * latent32, axis=-1, keepdims=True) + 1e-06)
-        * kv_gain
-    ).astype(jnp.bfloat16)
-    key_rot = rotate(rope_key[0], positions).astype(jnp.bfloat16)
-    packed = jnp.concatenate([latent_n] + [key_rot] * (LANES // rope), axis=1)
-    turned = rotate(queries[0, :, :, NOPE:], positions[:, None]).astype(jnp.bfloat16)
-    content = queries[0, :, :, :NOPE].reshape(tok, n, hn, NOPE).transpose(1, 2, 0, 3)
-    tiles = -(-hn * rope // LANES)
-    turned = turned.reshape(tok, n, hn * rope)
-    turned = jnp.pad(turned, ((0, 0), (0, 0), (0, tiles * LANES - hn * rope)))
-    turned = turned.reshape(tok, n, tiles, LANES).transpose(1, 2, 0, 3)
-    q = jnp.concatenate([content, turned], axis=1)
+    q = jnp.transpose(queries[0], (1, 2, 0))
+    key = jnp.transpose(rope_key[0])
+    table = jnp.asarray(rotation_table(n * tok, rope))
 
     d_in, cols = out_weight.shape
     part = d_in // g
@@ -334,22 +352,23 @@
     xn = max(nx - 1, 1)
     gn = max(g - 1, 1)
     vmem = pl.BlockSpec(memory_space=pltpu.VMEM)
+    hbm = pl.BlockSpec(memory_space=pltpu.HBM)
     out = pl.pallas_call(
         functools.partial(kernel, n, g, nx, hn, rope, width**-0.5, chunks),
         out_shape=jax.ShapeDtypeStruct((tok, cols * dp), bf),
-        in_specs=[vmem, vmem, vmem, pl.BlockSpec(memory_space=pltpu.HBM)],
+        in_specs=[hbm, vmem, vmem, vmem, vmem, hbm, hbm],
         out_specs=vmem,
         scratch_shapes=[
-            pltpu.VMEM((n, hn + tiles, tok, LANES), bf),
+            pltpu.VMEM((n, hn, width, tok), bf),
             pltpu.VMEM((n, tok, latw + LANES), bf),
             pltpu.VMEM((kv_weight.shape[0] * dp, kcols), bf),
             pltpu.VMEM((dp, d_in, cols), bf),
             pltpu.VMEM((hn, n * tok, NOPE + LANES), bf),
-            pltpu.VMEM((hn, n * tok, VD), bf),
+            pltpu.VMEM((hn, VD, n * tok), bf),
             pltpu.VMEM((n, tok, hn * VD), bf),
             pltpu.VMEM((n, tok, hn * VD), bf),
             pltpu.VMEM((tok, cols * dp), jnp.float32),
-            dma((5,)),
+            dma((3,)),
             dma((n,)), dma((n,)), dma((n,)), dma((n,)),
             dma((n,)), dma((n,)), dma((n,)), dma((n,)),
             dma((xn,)), dma((xn,)), dma((nx,)), dma((nx,)),
@@ -359,9 +378,9 @@
             dma(()), dma(()),
         ],
         compiler_params=pltpu.CompilerParams(
-            collective_id=0, has_side_effects=True, vmem_limit_bytes=56 * 1024 * 1024
+            collective_id=0, has_side_effects=True, vmem_limit_bytes=28 * 1024 * 1024
         ),
-    )(q, packed, kv_weight, out_weight)
+    )(q, kv_latent[0], key, kv_gain[None], table, kv_weight, out_weight)
     return out[None]
 
 

time: 75.9 us -> 73.3 us (0.966)
  Pallas kernels: 68.7 us -> 65.3 us
  local copies, waits for them, and re-layouts: 5.14 us -> 7.67 us
  other arithmetic: 1.62 us -> 0 us
    unnamed x6 -> x15, local copies, waits for them, and re-layouts: 2.78 us -> 7.67 us
    pallas_call x1, Pallas kernels: 68.7 us -> 65.3 us  [body(): pl.pallas_call(functools.partial(kernel, n, g, nx, hn, rope, width ** (-0...]
    squeeze x1 -> x0, local copies, waits for them, and re-layouts: 1 us -> none  [body(): queries[0, :, :, NOPE:]]
    concatenate x2 -> x0, other arithmetic: 0.98 us -> none  [the longest x1 0.96 us: body(): q = jnp.concatenate([content, turned], axis=1)]
    concatenate x1 -> x0, local copies, waits for them, and re-layouts: 0.78 us -> none  [body(): packed = jnp.concatenate([latent_n] + [key_rot] * (LANES // rope), axis=1)]
where the time goes in v2:
time: 73.3 us; the launch traced here: 73 us
  Pallas kernels  65.3 us (89%)
  local copies, waits for them, and re-layouts  7.67 us (10%)
    pallas_call x1, Pallas kernels, body(): pl.pallas_call(functools.partial(kernel, n, g, nx, hn, rope, width ** (-0...  65.3 us
    unnamed x15, local copies, waits for them, and re-layouts  7.67 us

profile of v2, /device:TPU:0, one launch (start us, length us, event | category | flops | bytes accessed | tf_op | source)
XLA Modules:
  0.0 73.0 jit_solution(6469530505108295315)
XLA Ops:
  0.0 0.0 copy-start
  0.0 1.6 %copy-done = bf16[2048,512]{1,0:T(8,128)(2,1)S(1)} copy-done((bf16[2048,512]{1,0:T(8,128)(2,1)S(1)}, bf16[2048,512]{1,0:T(8,128)(2,1)}, u32[]{:S(2)}) %copy-start) | copy-done | bytes 2097176
  1.6 0.0 copy-start.1
  1.6 1.1 %copy-done.1 = bf16[1,128,16,192]{1,3,2,0:T(8,128)(2,1)S(1)} copy-done((bf16[1,128,16,192]{1,3,2,0:T(8,128)(2,1)S(1)}, bf16[1,128,16,192]{1,3,2,0:T(8,128)(2,1)}, u32[]{:S(2)}) %copy-start.1) | copy-done | bytes 786456
  2.7 0.0 copy-start.2
  2.7 0.9 %copy-done.2 = bf16[128,1024]{1,0:T(8,128)(2,1)S(1)} copy-done((bf16[128,1024]{1,0:T(8,128)(2,1)S(1)}, bf16[128,1024]{1,0:T(8,128)(2,1)}, u32[]{:S(2)}) %copy-start.2) | copy-done | bytes 262168
  3.7 0.0 copy-start.3
  3.7 0.9 %copy-done.3 = bf16[1,128,512]{2,1,0:T(8,128)(2,1)S(1)} copy-done((bf16[1,128,512]{2,1,0:T(8,128)(2,1)S(1)}, bf16[1,128,512]{2,1,0:T(8,128)(2,1)}, u32[]{:S(2)}) %copy-start.3) | copy-done | bytes 131096
  4.6 0.0 copy-start.4
  4.6 0.9 %copy-done.4 = f32[2,32,512]{2,1,0:T(8,128)S(1)} copy-done((f32[2,32,512]{2,1,0:T(8,128)S(1)}, f32[2,32,512]{2,1,0:T(8,128)}, u32[]{:S(2)}) %copy-start.4) | copy-done | bytes 131096
  5.5 0.0 copy-start.5
  5.5 0.7 copy-done.5
  6.2 0.0 copy-start.6
  6.2 0.7 copy-done.6
  6.9 65.3 %shard_map.73 = bf16[128,2048]{1,0:T(8,128)(2,1)S(1)} custom-call(bf16[16,192,128]{2,1,0:T(8,128)(2,1)S(1)} %bitcast.10, bf16[128,512]{1,0:T(8,128)(2,1)S(1)} %bitcast.11, bf16[64,128]{1,0:T(8,128)(2,1)S(1)} %bitcast.12, f32[1,512]{1,0:T(1,128)S(1)} %bitcast.13, f32[2,32,512]{2,1,0:T(8,128)S(1)} %copy-done.4, bf16[128,1024]{1,0:T(8,128)(2,1)S(1)} %copy-done.2, ...), custom_call_target="tpu_custom_call" | custom-call | tf_op jit(solution)/shard_map/pallas_call | solution.py:356
  72.2 0.8 %copy.9 = bf16[1,128,2048]{2,1,0:T(8,128)(2,1)} copy(bf16[1,128,2048]{2,1,0:T(8,128)(2,1)S(1)} %bitcast.9) | data formatting | bytes 1048576
Async XLA Ops:
  0.0 1.6 %copy-start = (bf16[2048,512]{1,0:T(8,128)(2,1)S(1)}, bf16[2048,512]{1,0:T(8,128)(2,1)}, u32[]{:S(2)}) copy-start(bf16[2048,512]{1,0:T(8,128)(2,1)} %w_ref.1) | copy-start | bytes 6291460
  1.6 1.1 %copy-start.1 = (bf16[1,128,16,192]{1,3,2,0:T(8,128)(2,1)S(1)}, bf16[1,128,16,192]{1,3,2,0:T(8,128)(2,1)}, u32[]{:S(2)}) copy-start(bf16[1,128,16,192]{1,3,2,0:T(8,128)(2,1)} %param.7) | copy-start | bytes 2359300
  2.7 0.9 %copy-start.2 = (bf16[128,1024]{1,0:T(8,128)(2,1)S(1)}, bf16[128,1024]{1,0:T(8,128)(2,1)}, u32[]{:S(2)}) copy-start(bf16[128,1024]{1,0:T(8,128)(2,1)} %kvw_ref.1) | copy-start | bytes 786436
  3.7 0.9 %copy-start.3 = (bf16[1,128,512]{2,1,0:T(8,128)(2,1)S(1)}, bf16[1,128,512]{2,1,0:T(8,128)(2,1)}, u32[]{:S(2)}) copy-start(bf16[1,128,512]{2,1,0:T(8,128)(2,1)} %param.8) | copy-start | bytes 393220
  4.6 0.9 %copy-start.4 = (f32[2,32,512]{2,1,0:T(8,128)S(1)}, f32[2,32,512]{2,1,0:T(8,128)}, u32[]{:S(2)}) copy-start(f32[2,32,512]{2,1,0:T(8,128)} %constant.2.clone.table_ref) | copy-start | bytes 393220
  5.5 0.7 copy-start.5
  6.2 0.7 copy-start.6

commit v3 on v2

--- a/solution.py
+++ b/solution.py
@@ -14,6 +14,7 @@
 LANES = 128
 CORES = 2
 CHUNKS = 8
+LEAD = 3
 MESH = pl.DeviceIdType.MESH
 
 
@@ -142,9 +143,6 @@
         to = target(o)
         return remote(q_ref.at[pl.ds(to * hn, hn)], qbuf.at[me], q_s.at[o], q_r.at[o], {"sp": to})
 
-    for o in range(1, n):
-        q_copy(o).start()
-
     def w_rows(yy, ch):
         return pl.ds(pl.multiple_of(yy * part + ch * crow, crow), crow)
 
@@ -166,12 +164,21 @@
         ref = wfull.at[lax.rem(x + nx - o, nx) * CORES + c, w_rows(lax.rem(y + g - p, g), ch)]
         return remote(ref, ref, wc_s.at[o - 1, p, ch], wc_r.at[o - 1, p, ch], partner)
 
-    for ch in range(chunks):
-        for o in range(1, nx):
-            w_x(o, ch).start()
     w_own = remote(w_ref, wfull.at[dp], wo_s, wo_r, partner)
     w_own.start()
 
+    def start_queries():
+        for o in range(1, n):
+            q_copy(o).start()
+
+    def take_kv():
+        for o in range(1, nx):
+            kv_x(o).wait_recv()
+            kv_core(o).start()
+        for ch in range(min(LEAD, chunks)):
+            for o in range(1, nx):
+                w_x(o, ch).start()
+
     for k in range(1, n):
         @pl.when(me - k >= 0)
         def _():
@@ -189,9 +196,11 @@
             def _():
                 to_left(k, lat.at[me + k]).start()
 
-    for o in range(1, nx):
-        kv_x(o).wait_recv()
-        kv_core(o).start()
+        if k == n - 1:
+            start_queries()
+        if k == 1:
+            take_kv()
+
     own_k.wait()
     for o in range(nx):
         kv_core(o).wait_recv()
@@ -213,6 +222,11 @@
     def pass_x(ch):
         for o in range(1, nx):
             w_x(o, ch).wait_recv()
+
+            @pl.when(ch + LEAD < chunks)
+            def _():
+                w_x(o, ch + LEAD).start()
+
             for p in range(1, g):
                 w_y(o, p, ch).start()
             w_c(o, 0, ch).start()
@@ -242,9 +256,9 @@
             s = last if extent == step else jnp.concatenate([s[: extent - step], last], axis=0)
             top = jnp.max(s, axis=0, keepdims=True)
             e = jnp.exp2((s - top) * (scale * math.log2(math.e)))
-            total = jnp.sum(e, axis=0, keepdims=True)
-            o = jnp.dot(vbuf[h, :, :extent], e.astype(jnp.bfloat16), preferred_element_type=jnp.float32)
-            attsend[j, :, h * VD : (h + 1) * VD] = (o / total).T.astype(jnp.bfloat16)
+            p = (e * (1.0 / jnp.sum(e, axis=0, keepdims=True))).astype(jnp.bfloat16)
+            o = jnp.dot(vbuf[h, :, :extent], p, preferred_element_type=jnp.float32)
+            attsend[j, :, h * VD : (h + 1) * VD] = o.T.astype(jnp.bfloat16)
 
     def attention(j):
         for v in range(variants):

time: 73.3 us -> 59.9 us (0.82)
  Pallas kernels: 65.3 us -> 51.9 us
    pallas_call x1, Pallas kernels: 65.3 us -> 51.9 us  [body(): pl.pallas_call(functools.partial(kernel, n, g, nx, hn, rope, width ** (-0...]
where the time goes in v3:
time: 59.9 us; the launch traced here: 59.6 us
  Pallas kernels  51.9 us (87%)
  local copies, waits for them, and re-layouts  7.67 us (13%)
    pallas_call x1, Pallas kernels, body(): pl.pallas_call(functools.partial(kernel, n, g, nx, hn, rope, width ** (-0...  51.9 us
    unnamed x15, local copies, waits for them, and re-layouts  7.67 us

profile of v3, /device:TPU:0, one launch (start us, length us, event | category | flops | bytes accessed | tf_op | source)
XLA Modules:
  0.0 59.6 jit_solution(8873120649703272149)
XLA Ops:
  0.0 0.0 copy-start
  0.0 1.6 %copy-done = bf16[2048,512]{1,0:T(8,128)(2,1)S(1)} copy-done((bf16[2048,512]{1,0:T(8,128)(2,1)S(1)}, bf16[2048,512]{1,0:T(8,128)(2,1)}, u32[]{:S(2)}) %copy-start) | copy-done | bytes 2097176
  1.6 0.0 copy-start.1
  1.6 1.1 %copy-done.1 = bf16[1,128,16,192]{1,3,2,0:T(8,128)(2,1)S(1)} copy-done((bf16[1,128,16,192]{1,3,2,0:T(8,128)(2,1)S(1)}, bf16[1,128,16,192]{1,3,2,0:T(8,128)(2,1)}, u32[]{:S(2)}) %copy-start.1) | copy-done | bytes 786456
  2.7 0.0 copy-start.2
  2.7 0.9 %copy-done.2 = bf16[128,1024]{1,0:T(8,128)(2,1)S(1)} copy-done((bf16[128,1024]{1,0:T(8,128)(2,1)S(1)}, bf16[128,1024]{1,0:T(8,128)(2,1)}, u32[]{:S(2)}) %copy-start.2) | copy-done | bytes 262168
  3.7 0.0 copy-start.3
  3.7 0.9 %copy-done.3 = bf16[1,128,512]{2,1,0:T(8,128)(2,1)S(1)} copy-done((bf16[1,128,512]{2,1,0:T(8,128)(2,1)S(1)}, bf16[1,128,512]{2,1,0:T(8,128)(2,1)}, u32[]{:S(2)}) %copy-start.3) | copy-done | bytes 131096
  4.6 0.0 copy-start.4
  4.6 0.9 %copy-done.4 = f32[2,32,512]{2,1,0:T(8,128)S(1)} copy-done((f32[2,32,512]{2,1,0:T(8,128)S(1)}, f32[2,32,512]{2,1,0:T(8,128)}, u32[]{:S(2)}) %copy-start.4) | copy-done | bytes 131096
  5.5 0.0 copy-start.5
  5.5 0.7 %copy-done.5 = bf16[1,128,64]{1,2,0:T(8,128)(2,1)S(1)} copy-done((bf16[1,128,64]{1,2,0:T(8,128)(2,1)S(1)}, bf16[1,128,64]{1,2,0:T(8,128)(2,1)}, u32[]{:S(2)}) %copy-start.5) | copy-done | bytes 16408
  6.2 0.0 copy-start.6
  6.2 0.7 %copy-done.6 = f32[512]{0:T(512)S(1)} copy-done((f32[512]{0:T(512)S(1)}, f32[512]{0:T(512)}, u32[]{:S(2)}) %copy-start.6) | copy-done | bytes 2072
  6.9 51.9 %shard_map.73 = bf16[128,2048]{1,0:T(8,128)(2,1)S(1)} custom-call(bf16[16,192,128]{2,1,0:T(8,128)(2,1)S(1)} %bitcast.10, bf16[128,512]{1,0:T(8,128)(2,1)S(1)} %bitcast.11, bf16[64,128]{1,0:T(8,128)(2,1)S(1)} %bitcast.12, f32[1,512]{1,0:T(1,128)S(1)} %bitcast.13, f32[2,32,512]{2,1,0:T(8,128)S(1)} %copy-done.4, bf16[128,1024]{1,0:T(8,128)(2,1)S(1)} %copy-done.2, ...), custom_call_target="tpu_custom_call" | custom-call | tf_op jit(solution)/shard_map/pallas_call | solution.py:370
  58.8 0.8 %copy.9 = bf16[1,128,2048]{2,1,0:T(8,128)(2,1)} copy(bf16[1,128,2048]{2,1,0:T(8,128)(2,1)S(1)} %bitcast.9) | data formatting | bytes 1048576
Async XLA Ops:
  0.0 1.6 %copy-start = (bf16[2048,512]{1,0:T(8,128)(2,1)S(1)}, bf16[2048,512]{1,0:T(8,128)(2,1)}, u32[]{:S(2)}) copy-start(bf16[2048,512]{1,0:T(8,128)(2,1)} %w_ref.1) | copy-start | bytes 6291460
  1.6 1.1 %copy-start.1 = (bf16[1,128,16,192]{1,3,2,0:T(8,128)(2,1)S(1)}, bf16[1,128,16,192]{1,3,2,0:T(8,128)(2,1)}, u32[]{:S(2)}) copy-start(bf16[1,128,16,192]{1,3,2,0:T(8,128)(2,1)} %param.7) | copy-start | bytes 2359300
  2.7 0.9 %copy-start.2 = (bf16[128,1024]{1,0:T(8,128)(2,1)S(1)}, bf16[128,1024]{1,0:T(8,128)(2,1)}, u32[]{:S(2)}) copy-start(bf16[128,1024]{1,0:T(8,128)(2,1)} %kvw_ref.1) | copy-start | bytes 786436
  3.7 0.9 %copy-start.3 = (bf16[1,128,512]{2,1,0:T(8,128)(2,1)S(1)}, bf16[1,128,512]{2,1,0:T(8,128)(2,1)}, u32[]{:S(2)}) copy-start(bf16[1,128,512]{2,1,0:T(8,128)(2,1)} %param.8) | copy-start | bytes 393220
  4.6 0.9 %copy-start.4 = (f32[2,32,512]{2,1,0:T(8,128)S(1)}, f32[2,32,512]{2,1,0:T(8,128)}, u32[]{:S(2)}) copy-start(f32[2,32,512]{2,1,0:T(8,128)} %constant.2.clone.table_ref) | copy-start | bytes 393220
  5.5 0.7 %copy-start.5 = (bf16[1,128,64]{1,2,0:T(8,128)(2,1)S(1)}, bf16[1,128,64]{1,2,0:T(8,128)(2,1)}, u32[]{:S(2)}) copy-start(bf16[1,128,64]{1,2,0:T(8,128)(2,1)} %param.9) | copy-start | bytes 49156
  6.2 0.7 %copy-start.6 = (f32[512]{0:T(512)S(1)}, f32[512]{0:T(512)}, u32[]{:S(2)}) copy-start(f32[512]{0:T(512)} %param.10) | copy-start | bytes 6148
